TPU v7x, 128 devices: a whole 4x4x4 slice. The times are simulated.
128 devices in a mesh: sp: 32 (over z, y, core), tp: 4 (over x).
Axes of the slice: x: 4, y: 4, z: 4, core: 2. Of those that a mesh axis runs over, the one named last changes fastest.
Arguments:
- tokens: bfloat16 [4, 2048, 1024], P(None, 'sp', 'tp'), may hold values from -6 to 6
- norm_gain: float32 [4, 1024], replicated, may hold values from 0.1 to 1.9
- val_weight: bfloat16 [4, 1024, 512], P(None, 'sp', 'tp'), may hold values from -0.1875 to 0.1875
- gate_weight: bfloat16 [4, 1024, 512], P(None, 'sp', 'tp'), may hold values from -0.1875 to 0.1875
- conv_taps: float32 [4, 31, 512], P(None, None, 'tp'), may hold values from -1 to 1
- conv_bias: float32 [4, 512], P(None, 'tp'), may hold values from -3 to 3
- ln_gain: float32 [4, 512], P(None, 'tp'), may hold values from 0.1 to 1.9
- ln_shift: float32 [4, 512], P(None, 'tp'), may hold values from -3 to 3
- out_weight: bfloat16 [4, 512, 1024], P(None, 'tp', 'sp'), may hold values from -0.25 to 0.25
Outputs:
- stream: bfloat16 [4, 2048, 1024], P(None, 'sp', 'tp')
All inputs are finite; a program needn't handle non-finite values.
Results may differ from a plain program's by a relative error of at most 0.02.
Values may be sent and summed in bfloat16 or wider, within the bound.
A program may use at most 64 MiB of HBM per device.

v0:
```python
from functools import partial
import jax
import jax.numpy as jnp
from jax import lax
from jax.sharding import PartitionSpec as P

LAYERS = 4
epsilon = 1e-06


def over_all(shard, axis, dim, absorb, state):
    everything = jax.tree.map(lambda a: lax.all_gather(a, axis, axis=dim, tiled=True), shard)
    return absorb(state, everything, jnp.int32(0))


def with_halo(shard, sides, width, wrap):
    for axis, dim in sides:
        size, length = (lax.axis_size(axis), shard.shape[dim])
        up = [(i, (i + 1) % size) for i in range(size if wrap else size - 1)]
        down = [(j, i) for i, j in up]
        last = lax.slice_in_dim(shard, length - width, length, axis=dim)
        initial = lax.slice_in_dim(shard, 0, width, axis=dim)
        before = lax.ppermute(last, axis, up)
        after = lax.ppermute(initial, axis, down)
        shard = jnp.concatenate([before, shard, after], axis=dim)
    return shard


def together(arrays, axis):
    ends = [0]
    for a in arrays:
        ends.append(ends[-1] + a.size)
    subtotal = lax.psum(jnp.concatenate([a.ravel() for a in arrays]), axis)
    return tuple((subtotal[b:e].reshape(a.shape) for a, b, e in zip(arrays, ends, ends[1:])))


def on_whole(shard, axis, dim, work):
    return work(lax.all_gather(shard, axis, axis=dim, tiled=True), jnp.int32(0))


def depthwise(padded, tap_weights, length):
    running = padded[:, 0:length] * tap_weights[0]
    for tap_idx in range(1, tap_weights.shape[0]):
        running = running + padded[:, tap_idx : tap_idx + length] * tap_weights[tap_idx]
    return running


def add_rows(left_rows, running, shard_piece, offset):
    columns = lax.dynamic_slice_in_dim(left_rows, offset, shard_piece.shape[0], 1)
    return running + jnp.dot(columns, shard_piece, preferred_element_type=jnp.float32)


def add_both(left_rows, totals, pieces, offset):
    return (
        add_rows(left_rows, totals[0], pieces[0], offset),
        add_rows(left_rows, totals[1], pieces[1], offset),
    )


def project_rows(left_rows, shard_piece, offset):
    return jnp.dot(left_rows, shard_piece, preferred_element_type=jnp.float32)


def shards(
    tokens, norm_gain, val_weight, gate_weight, conv_taps, conv_bias, ln_gain, ln_shift, out_weight
):
    stream = tokens
    num_seqs = tokens.shape[0]
    local_len = tokens.shape[1]
    chan_width = val_weight.shape[2]
    all_channels = chan_width * lax.axis_size("tp")
    half_width = conv_taps.shape[1] // 2
    for layer_idx in range(LAYERS):
        gathered = lax.all_gather(stream, "tp", axis=2, tiled=True)
        widened = gathered.astype(jnp.float32)
        scaled = widened * lax.rsqrt(jnp.mean(widened * widened, axis=-1, keepdims=True) + epsilon)
        normed = (scaled * norm_gain[layer_idx]).astype(jnp.bfloat16)
        tok_rows = normed.reshape(-1, normed.shape[2])
        zeroed = jnp.zeros((tok_rows.shape[0], chan_width), jnp.float32)
        values, gates = over_all(
            (val_weight[layer_idx], gate_weight[layer_idx]),
            "sp",
            0,
            partial(add_both, tok_rows),
            (zeroed, zeroed),
        )
        gated = (
            (values * jax.nn.sigmoid(gates))
            .astype(jnp.bfloat16)
            .reshape(num_seqs, local_len, chan_width)
        )
        padded = with_halo(gated, (("sp", 1),), half_width, False)
        convolved = (
            depthwise(padded.astype(jnp.float32), conv_taps[layer_idx], local_len)
            + conv_bias[layer_idx]
        )
        first_sum, second_sum = together(
            (jnp.sum(convolved, axis=-1), jnp.sum(convolved * convolved, axis=-1)), "tp"
        )
        mean_val = (first_sum / all_channels)[..., None]
        spread = (second_sum / all_channels)[..., None] - mean_val * mean_val
        centered = convolved - mean_val
        normalized = (
            centered * lax.rsqrt(spread + epsilon) * ln_gain[layer_idx] + ln_shift[layer_idx]
        )
        activated = jax.nn.silu(normalized).astype(jnp.bfloat16).reshape(-1, chan_width)
        partial_terms = on_whole(out_weight[layer_idx], "sp", 1, partial(project_rows, activated))
        full_width = partial_terms.shape[1]
        summed = lax.psum_scatter(
            partial_terms.reshape(num_seqs, local_len, full_width).astype(jnp.bfloat16),
            "tp",
            scatter_dimension=2,
            tiled=True,
        ).astype(jnp.float32)
        stream = (stream.astype(jnp.float32) + summed).astype(jnp.bfloat16)
    return stream


def solution(mesh):
    return jax.shard_map(
        shards,
        mesh=mesh,
        in_specs=(
            P(None, "sp", "tp"),
            P(),
            P(None, "sp", "tp"),
            P(None, "sp", "tp"),
            P(None, None, "tp"),
            P(None, "tp"),
            P(None, "tp"),
            P(None, "tp"),
            P(None, "tp", "sp"),
        ),
        out_specs=P(None, "sp", "tp"),
        check_vma=False,
    )
```

profile of v0, /device:TPU:0, one launch (start us, length us, event | category | flops | bytes accessed | tf_op | source)
XLA Modules:
  0.0 455.9 jit_solution(18299880186058381866)
XLA Ops:
  7.4 13.5 %all_gather.48 = bf16[4,64,1024]{2,1,0:T(8,128)(2,1)S(1)} all-gather(bf16[4,64,256]{2,1,0:T(8,128)(2,1)} %param.9), channel_id=1, replica_groups=mesh['sp'=32,'tp'=4] {'tp'}, dimensions={2}, use_global_device_ids=true | all-gather | bytes 655360 | tf_op jit(solution)/shard_map/all_gather | solution.py:74
  21.6 26.5 %all-gather = bf16[1,1024,128]{2,1,0:T(8,128)(2,1)S(1)} all-gather(bf16[1,32,128]{2,1,0:T(8,128)(2,1)S(1)} %get-tuple-element.155), channel_id=2, replica_groups=mesh['sp'=32,'tp'=4] {'sp'}, dimensions={1}, use_global_device_ids=true | all-gather | bytes 270336 | tf_op jit(solution)/shard_map/all_gather | solution.py:12
  48.1 24.3 %all-gather.1 = bf16[1,1024,128]{2,1,0:T(8,128)(2,1)S(1)} all-gather(bf16[1,32,128]{2,1,0:T(8,128)(2,1)S(1)} %get-tuple-element.151), channel_id=3, replica_groups=mesh['sp'=32,'tp'=4] {'sp'}, dimensions={1}, use_global_device_ids=true | all-gather | bytes 270336 | tf_op jit(solution)/shard_map/all_gather | solution.py:12
  73.2 2.3 collective-permute-start
  75.5 1.3 collective-permute-start.1
  78.3 26.7 %all-gather.2 = bf16[1,128,1024]{1,2,0:T(8,128)(2,1)S(1)} all-gather(bf16[1,128,32]{1,2,0:T(8,128)(2,1)S(1)} %get-tuple-element.157), channel_id=4, replica_groups=mesh['sp'=32,'tp'=4] {'sp'}, dimensions={2}, use_global_device_ids=true | all-gather | bytes 270336 | tf_op jit(solution)/shard_map/all_gather | solution.py:38
  105.7 10.7 %psum.28 = f32[512]{0:T(512)S(1)} all-reduce(f32[512]{0:T(512)S(1)} %pad_maximum_fusion), channel_id=1, replica_groups=mesh['sp'=32,'tp'=4] {'tp'}, use_global_device_ids=true, to_apply=%region_3.0 | all-reduce | flops 512 | bytes 4096 | tf_op jit(solution)/shard_map/psum | solution.py:33
  116.6 1.2 convolution_convert_fusion.3
  117.8 23.1 %all-gather.3 = bf16[1,1024,128]{2,1,0:T(8,128)(2,1)S(1)} all-gather(bf16[1,32,128]{2,1,0:T(8,128)(2,1)S(1)} %get-tuple-element.154), channel_id=5, replica_groups=mesh['sp'=32,'tp'=4] {'sp'}, dimensions={1}, use_global_device_ids=true | all-gather | bytes 270336 | tf_op jit(solution)/shard_map/all_gather | solution.py:12
  140.9 23.9 %all-gather.4 = bf16[1,1024,128]{2,1,0:T(8,128)(2,1)S(1)} all-gather(bf16[1,32,128]{2,1,0:T(8,128)(2,1)S(1)} %get-tuple-element.150), channel_id=6, replica_groups=mesh['sp'=32,'tp'=4] {'sp'}, dimensions={1}, use_global_device_ids=true | all-gather | bytes 270336 | tf_op jit(solution)/shard_map/all_gather | solution.py:12
  165.8 13.5 %all_gather.52 = bf16[4,64,1024]{2,1,0:T(8,128)(2,1)S(1)} all-gather(bf16[4,64,256]{2,1,0:T(8,128)(2,1)S(1)} %add_convert_fusion.3), channel_id=1, replica_groups=mesh['sp'=32,'tp'=4] {'tp'}, dimensions={2}, use_global_device_ids=true | all-gather | bytes 655360 | tf_op jit(solution)/shard_map/all_gather | solution.py:74
  180.3 1.3 collective-permute-start.2
  181.6 1.3 collective-permute-start.3
  182.9 28.4 %all-gather.5 = bf16[1,128,1024]{1,2,0:T(8,128)(2,1)S(1)} all-gather(bf16[1,128,32]{1,2,0:T(8,128)(2,1)S(1)} %get-tuple-element.158), channel_id=7, replica_groups=mesh['sp'=32,'tp'=4] {'sp'}, dimensions={2}, use_global_device_ids=true | all-gather | bytes 270336 | tf_op jit(solution)/shard_map/all_gather | solution.py:38
  212.0 7.7 %psum.29 = f32[512]{0:T(512)S(1)} all-reduce(f32[512]{0:T(512)S(1)} %pad_maximum_fusion.1), channel_id=1, replica_groups=mesh['sp'=32,'tp'=4] {'tp'}, use_global_device_ids=true, to_apply=%region_8.9 | all-reduce | flops 512 | bytes 4096 | tf_op jit(solution)/shard_map/psum | solution.py:33
  221.2 22.6 %all-gather.6 = bf16[1,1024,128]{2,1,0:T(8,128)(2,1)S(1)} all-gather(bf16[1,32,128]{2,1,0:T(8,128)(2,1)S(1)} %get-tuple-element.156), channel_id=8, replica_groups=mesh['sp'=32,'tp'=4] {'sp'}, dimensions={1}, use_global_device_ids=true | all-gather | bytes 270336 | tf_op jit(solution)/shard_map/all_gather | solution.py:12
  243.7 24.3 %all-gather.7 = bf16[1,1024,128]{2,1,0:T(8,128)(2,1)S(1)} all-gather(bf16[1,32,128]{2,1,0:T(8,128)(2,1)S(1)} %get-tuple-element.152), channel_id=9, replica_groups=mesh['sp'=32,'tp'=4] {'sp'}, dimensions={1}, use_global_device_ids=true | all-gather | bytes 270336 | tf_op jit(solution)/shard_map/all_gather | solution.py:12
  269.0 12.9 %all_gather.56 = bf16[4,64,1024]{2,1,0:T(8,128)(2,1)S(1)} all-gather(bf16[4,64,256]{2,1,0:T(8,128)(2,1)S(1)} %add_convert_fusion.2), channel_id=1, replica_groups=mesh['sp'=32,'tp'=4] {'tp'}, dimensions={2}, use_global_device_ids=true | all-gather | bytes 655360 | tf_op jit(solution)/shard_map/all_gather | solution.py:74
  282.9 1.3 collective-permute-start.4
  284.2 1.3 collective-permute-start.5
  285.5 27.6 %all-gather.8 = bf16[1,128,1024]{1,2,0:T(8,128)(2,1)S(1)} all-gather(bf16[1,128,32]{1,2,0:T(8,128)(2,1)S(1)} %get-tuple-element.160), channel_id=10, replica_groups=mesh['sp'=32,'tp'=4] {'sp'}, dimensions={2}, use_global_device_ids=true | all-gather | bytes 270336 | tf_op jit(solution)/shard_map/all_gather | solution.py:38
  313.9 9.9 %psum.30 = f32[512]{0:T(512)S(1)} all-reduce(f32[512]{0:T(512)S(1)} %pad_maximum_fusion.2), channel_id=1, replica_groups=mesh['sp'=32,'tp'=4] {'tp'}, use_global_device_ids=true, to_apply=%region_13.14 | all-reduce | flops 512 | bytes 4096 | tf_op jit(solution)/shard_map/psum | solution.py:33
  324.0 1.2 convolution_convert_fusion.1
  325.3 23.1 %all-gather.9 = bf16[1,1024,128]{2,1,0:T(8,128)(2,1)S(1)} all-gather(bf16[1,32,128]{2,1,0:T(8,128)(2,1)S(1)} %get-tuple-element.153), channel_id=11, replica_groups=mesh['sp'=32,'tp'=4] {'sp'}, dimensions={1}, use_global_device_ids=true | all-gather | bytes 270336 | tf_op jit(solution)/shard_map/all_gather | solution.py:12
  348.3 24.0 %all-gather.10 = bf16[1,1024,128]{2,1,0:T(8,128)(2,1)S(1)} all-gather(bf16[1,32,128]{2,1,0:T(8,128)(2,1)S(1)} %get-tuple-element.149), channel_id=12, replica_groups=mesh['sp'=32,'tp'=4] {'sp'}, dimensions={1}, use_global_device_ids=true | all-gather | bytes 270336 | tf_op jit(solution)/shard_map/all_gather | solution.py:12
  373.3 13.5 %all_gather.60 = bf16[4,64,1024]{2,1,0:T(8,128)(2,1)S(1)} all-gather(bf16[4,64,256]{2,1,0:T(8,128)(2,1)S(1)} %add_convert_fusion.1), channel_id=1, replica_groups=mesh['sp'=32,'tp'=4] {'tp'}, dimensions={2}, use_global_device_ids=true | all-gather | bytes 655360 | tf_op jit(solution)/shard_map/all_gather | solution.py:74
  387.8 1.3 collective-permute-start.6
  389.1 1.3 collective-permute-start.7
  390.4 28.2 %all-gather.11 = bf16[1,128,1024]{1,2,0:T(8,128)(2,1)S(1)} all-gather(bf16[1,128,32]{1,2,0:T(8,128)(2,1)S(1)} %get-tuple-element.159), channel_id=13, replica_groups=mesh['sp'=32,'tp'=4] {'sp'}, dimensions={2}, use_global_device_ids=true | all-gather | bytes 270336 | tf_op jit(solution)/shard_map/all_gather | solution.py:38
  419.4 7.7 %psum.31 = f32[512]{0:T(512)S(1)} all-reduce(f32[512]{0:T(512)S(1)} %pad_maximum_fusion.3), channel_id=1, replica_groups=mesh['sp'=32,'tp'=4] {'tp'}, use_global_device_ids=true, to_apply=%region_18.19 | all-reduce | flops 512 | bytes 4096 | tf_op jit(solution)/shard_map/psum | solution.py:33
  428.5 19.3 %reduce-scatter.11.cloned.1.call-done = bf16[4,64,256]{2,1,0:T(8,128)(2,1)} async-done(((bf16[4,64,1024]{2,1,0:T(8,128)(2,1)}), bf16[4,64,256]{2,1,0:T(8,128)(2,1)}) %reduce-scatter.11.cloned.1.call-update) | async-done | bytes 131088 | tf_op jit(solution)/shard_map/reduce_scatter | solution.py:109
  447.7 1.6 add_convert_fusion
  (113 shorter events, 16.0 us)
Async XLA Ops:
  6.5 158.3 %reduce-scatter.5.cloned.1.call-start = ((), (), s32[]{:S(2)}) async-start(), calls=%async_computation.4 | async-start | bytes 655360 | tf_op jit(solution)/shard_map/reduce_scatter | solution.py:109
  20.9 0.8 copy-start.2
  21.6 26.5 %copy-start.3 = (bf16[4,32,128]{2,1,0:T(8,128)(2,1)S(1)}, bf16[4,32,128]{2,1,0:T(8,128)(2,1)}, u32[]{:S(2)}) copy-start(bf16[4,32,128]{2,1,0:T(8,128)(2,1)} %param.12) | copy-start | bytes 98308
  73.2 3.6 copy-start.1
  73.2 4.3 copy-start.4
  73.2 31.7 %collective-permute-start = (bf16[4,15,128]{2,1,0:T(8,128)(2,1)S(1)}, bf16[4,15,128]{2,1,0:T(8,128)(2,1)S(1)}, u32[]{:S(2)}, u32[]{:S(2)}) collective-permute-start(bf16[4,15,128]{2,1,0:T(8,128)(2,1)S(1)} %get-tuple-element.23), channel_id=1, source_target_pairs={{0,4},{4,8},{8,12},{12,16},{16,20},{20,24},{24,28},{28,32},{32,36}... | collective-permute-start | bytes 46088 | tf_op jit(solution)/shard_map/ppermute | solution.py:23
  75.5 29.4 %collective-permute-start.1 = (bf16[4,15,128]{2,1,0:T(8,128)(2,1)S(1)}, bf16[4,15,128]{2,1,0:T(8,128)(2,1)S(1)}, u32[]{:S(2)}, u32[]{:S(2)}) collective-permute-start(bf16[4,15,128]{2,1,0:T(8,128)(2,1)S(1)} %get-tuple-element.24), channel_id=1, source_target_pairs={{4,0},{8,4},{12,8},{16,12},{20,16},{24,20},{28,24},{32,28},{36,32}... | collective-permute-start | bytes 46088 | tf_op jit(solution)/shard_map/ppermute | solution.py:24
  76.9 0.7 copy-start.5
  77.5 0.7 copy-start.6
  77.6 0.7 copy-start.7
  117.8 150.3 %reduce-scatter.7.cloned.1.call-start = ((), (), s32[]{:S(2)}) async-start(), calls=%async_computation.5 | async-start | bytes 655360 | tf_op jit(solution)/shard_map/reduce_scatter | solution.py:109
  140.9 23.9 %copy-start = (bf16[4,64,256]{2,1,0:T(8,128)(2,1)S(1)}, bf16[4,64,256]{2,1,0:T(8,128)(2,1)}, u32[]{:S(2)}) copy-start(bf16[4,64,256]{2,1,0:T(8,128)(2,1)} %param.9) | copy-start | bytes 393220
  180.3 31.0 %collective-permute-start.2 = (bf16[4,15,128]{2,1,0:T(8,128)(2,1)S(1)}, bf16[4,15,128]{2,1,0:T(8,128)(2,1)S(1)}, u32[]{:S(2)}, u32[]{:S(2)}) collective-permute-start(bf16[4,15,128]{2,1,0:T(8,128)(2,1)S(1)} %get-tuple-element.21), channel_id=1, source_target_pairs={{0,4},{4,8},{8,12},{12,16},{16,20},{20,24},{24,28},{28,32},{32,36}... | collective-permute-start | bytes 46088 | tf_op jit(solution)/shard_map/ppermute | solution.py:23
  181.6 29.7 %collective-permute-start.3 = (bf16[4,15,128]{2,1,0:T(8,128)(2,1)S(1)}, bf16[4,15,128]{2,1,0:T(8,128)(2,1)S(1)}, u32[]{:S(2)}, u32[]{:S(2)}) collective-permute-start(bf16[4,15,128]{2,1,0:T(8,128)(2,1)S(1)} %get-tuple-element.22), channel_id=1, source_target_pairs={{4,0},{8,4},{12,8},{16,12},{20,16},{24,20},{28,24},{32,28},{36,32}... | collective-permute-start | bytes 46088 | tf_op jit(solution)/shard_map/ppermute | solution.py:24
  221.1 151.2 %reduce-scatter.9.cloned.1.call-start = ((), (), s32[]{:S(2)}) async-start(), calls=%async_computation.6 | async-start | bytes 655360 | tf_op jit(solution)/shard_map/reduce_scatter | solution.py:109
  282.9 30.3 %collective-permute-start.4 = (bf16[4,15,128]{2,1,0:T(8,128)(2,1)S(1)}, bf16[4,15,128]{2,1,0:T(8,128)(2,1)S(1)}, u32[]{:S(2)}, u32[]{:S(2)}) collective-permute-start(bf16[4,15,128]{2,1,0:T(8,128)(2,1)S(1)} %get-tuple-element.19), channel_id=1, source_target_pairs={{0,4},{4,8},{8,12},{12,16},{16,20},{20,24},{24,28},{28,32},{32,36}... | collective-permute-start | bytes 46088 | tf_op jit(solution)/shard_map/ppermute | solution.py:23
  284.2 29.0 %collective-permute-start.5 = (bf16[4,15,128]{2,1,0:T(8,128)(2,1)S(1)}, bf16[4,15,128]{2,1,0:T(8,128)(2,1)S(1)}, u32[]{:S(2)}, u32[]{:S(2)}) collective-permute-start(bf16[4,15,128]{2,1,0:T(8,128)(2,1)S(1)} %get-tuple-element.20), channel_id=1, source_target_pairs={{4,0},{8,4},{12,8},{16,12},{20,16},{24,20},{28,24},{32,28},{36,32}... | collective-permute-start | bytes 46088 | tf_op jit(solution)/shard_map/ppermute | solution.py:24
  325.2 122.5 %reduce-scatter.11.cloned.1.call-start = ((), (), s32[]{:S(2)}) async-start(), calls=%async_computation.7 | async-start | bytes 655360 | tf_op jit(solution)/shard_map/reduce_scatter | solution.py:109
  387.8 30.8 %collective-permute-start.6 = (bf16[4,15,128]{2,1,0:T(8,128)(2,1)S(1)}, bf16[4,15,128]{2,1,0:T(8,128)(2,1)S(1)}, u32[]{:S(2)}, u32[]{:S(2)}) collective-permute-start(bf16[4,15,128]{2,1,0:T(8,128)(2,1)S(1)} %get-tuple-element.17), channel_id=1, source_target_pairs={{0,4},{4,8},{8,12},{12,16},{16,20},{20,24},{24,28},{28,32},{32,36}... | collective-permute-start | bytes 46088 | tf_op jit(solution)/shard_map/ppermute | solution.py:23
  389.1 29.5 %collective-permute-start.7 = (bf16[4,15,128]{2,1,0:T(8,128)(2,1)S(1)}, bf16[4,15,128]{2,1,0:T(8,128)(2,1)S(1)}, u32[]{:S(2)}, u32[]{:S(2)}) collective-permute-start(bf16[4,15,128]{2,1,0:T(8,128)(2,1)S(1)} %get-tuple-element.18), channel_id=1, source_target_pairs={{4,0},{8,4},{12,8},{16,12},{20,16},{24,20},{28,24},{32,28},{36,32}... | collective-permute-start | bytes 46088 | tf_op jit(solution)/shard_map/ppermute | solution.py:24
Sparse Core Ops, SparseCore 0:
  117.9 18.4 reduce-scatter.4
  221.2 19.1 reduce-scatter.6
  325.3 18.5 reduce-scatter.8
  428.6 19.1 reduce-scatter.10
where the time goes:
time: 457 us; the launch traced here: 456 us
  blocking collectives  392 us (86%)
  waiting for transfers between devices  19.4 us (4%)
  between operations  13.5 us (3%)
  starting transfers between devices  11.4 us (2%)
  other arithmetic  8.4 us (2%)
  matrix products  7 us (2%)
    all_gather x8, blocking collectives, over_all(): lax.all_gather(a, axis, axis=dim, tiled=True)  192 us
    all_gather x4, blocking collectives, on_whole(): return work(lax.all_gather(shard, axis, axis=dim, tiled=True), jnp.int32(0))  111 us
    all_gather x4, blocking collectives, shards(): gathered = lax.all_gather(stream, 'tp', axis=2, tiled=True)  53.4 us
    psum x4, blocking collectives, together(): subtotal = lax.psum(jnp.concatenate([a.ravel() for a in arrays]), axis)  36.1 us
    reduce_scatter x4, waiting for transfers between devices, shards(): lax.psum_scatter(partial_terms.reshape(num_seqs, local_len, full_width).a...  19.4 us
  transfers between devices with their start and end apart: 12, of which 1 were waited for; matrix products, arithmetic and copies ran while one was open for 0% of the time, Pallas kernels for 0%

commit v1 on v0

--- a/solution.py
+++ b/solution.py
@@ -6,6 +6,28 @@
 
 LAYERS = 4
 epsilon = 1e-06
+
+
+def laid_out(tiles, dim):
+    shape = list(tiles.shape[1:])
+    shape[dim] *= tiles.shape[0]
+    return jnp.moveaxis(tiles, 0, dim).reshape(shape)
+
+
+def gather_around(x, axis, dim):
+    size = lax.axis_size(axis)
+    pairs = [(i, (i + 1) % size) for i in range(size)]
+    back = [(b, a) for a, b in pairs]
+    lower, upper = ([], [])
+    for lap in range(size - 1):
+        if lap % 2 == 0:
+            lower.append(lax.ppermute(lower[-1] if lower else x, axis, pairs))
+        else:
+            upper.append(lax.ppermute(upper[-1] if upper else x, axis, back))
+    pieces = jnp.stack([*lower[::-1], x, *upper])
+    shift = lax.axis_index(axis) - len(lower)
+    pieces = pieces[(jnp.arange(size) - shift) % size]
+    return laid_out(pieces, dim)
 
 
 def over_all(shard, axis, dim, absorb, state):
@@ -71,7 +93,7 @@
     all_channels = chan_width * lax.axis_size("tp")
     half_width = conv_taps.shape[1] // 2
     for layer_idx in range(LAYERS):
-        gathered = lax.all_gather(stream, "tp", axis=2, tiled=True)
+        gathered = gather_around(stream, "tp", 2)
         widened = gathered.astype(jnp.float32)
         scaled = widened * lax.rsqrt(jnp.mean(widened * widened, axis=-1, keepdims=True) + epsilon)
         normed = (scaled * norm_gain[layer_idx]).astype(jnp.bfloat16)

time: 457 us -> 512 us (1.12); the launches traced: 456 us -> 503 us
  waiting for transfers between devices: 19.4 us -> 83 us
  blocking collectives: 392 us -> 350 us
  starting transfers between devices: 11.4 us -> 27.9 us
  local copies, waits for them, and re-layouts: 4.25 us -> 12.3 us
    reduce_scatter x4, waiting for transfers between devices: 19.4 us -> 74.2 us  [shards(): lax.psum_scatter(partial_terms.reshape(num_seqs, local_len, full_width).a...]
    all_gather x4 -> x0, blocking collectives: 53.4 us -> none  [shards(): gathered = lax.all_gather(stream, 'tp', axis=2, tiled=True)]
    ppermute x0 -> x12, starting transfers between devices: none -> 13.5 us  [the longest x4 11.4 us: gather_around(): upper.append(lax.ppermute(upper[-1] if upper else x, axis, back))]
    ppermute x0 -> x12, waiting for transfers between devices: none -> 8.76 us  [the longest x8 8.75 us: gather_around(): lower.append(lax.ppermute(lower[-1] if lower else x, axis, pairs))]
    all_gather x8, blocking collectives: 192 us -> 200 us  [over_all(): lax.all_gather(a, axis, axis=dim, tiled=True)]
    psum x4, blocking collectives: 36.1 us -> 43.5 us  [together(): subtotal = lax.psum(jnp.concatenate([a.ravel() for a in arrays]), axis)]
  transfers between devices with their start and end apart: 12 -> 24, of which waited for: 1 -> 7; matrix products, arithmetic and copies ran while one was open for 0% -> 1% of each run, Pallas kernels for 0% -> 0%
where the time goes in v1:
time: 512 us; the launch traced here: 503 us
  blocking collectives  350 us (68%)
  waiting for transfers between devices  83 us (16%)
  starting transfers between devices  27.9 us (5%)
  between operations  13.9 us (3%)
  local copies, waits for them, and re-layouts  12.3 us (2%)
  other arithmetic  8.33 us (2%)
  matrix products  7.51 us (1%)
    all_gather x8, blocking collectives, over_all(): lax.all_gather(a, axis, axis=dim, tiled=True)  200 us
    all_gather x4, blocking collectives, on_whole(): return work(lax.all_gather(shard, axis, axis=dim, tiled=True), jnp.int32(0))  107 us
    reduce_scatter x4, waiting for transfers between devices, shards(): lax.psum_scatter(partial_terms.reshape(num_seqs, local_len, full_width).a...  74.2 us
    psum x4, blocking collectives, together(): subtotal = lax.psum(jnp.concatenate([a.ravel() for a in arrays]), axis)  43.5 us
    ppermute x4, starting transfers between devices, gather_around(): upper.append(lax.ppermute(upper[-1] if upper else x, axis, back))  11.4 us
  transfers between devices with their start and end apart: 24, of which 7 were waited for; matrix products, arithmetic and copies ran while one was open for 1% of the time, Pallas kernels for 0%

profile of v1, /device:TPU:0, one launch (start us, length us, event | category | flops | bytes accessed | tf_op | source)
XLA Modules:
  0.0 503.1 jit_solution(13409084615116185455)
XLA Ops:
  6.5 1.6 collective-permute-start
  8.1 1.6 collective-permute-start.2
  14.6 26.5 %all-gather = bf16[1,1024,128]{2,1,0:T(8,128)(2,1)S(1)} all-gather(bf16[1,32,128]{2,1,0:T(8,128)(2,1)S(1)} %get-tuple-element.153), channel_id=2, replica_groups=mesh['sp'=32,'tp'=4] {'sp'}, dimensions={1}, use_global_device_ids=true | all-gather | bytes 270336 | tf_op jit(solution)/shard_map/all_gather | solution.py:34
  41.5 24.4 %all-gather.1 = bf16[1,1024,128]{2,1,0:T(8,128)(2,1)S(1)} all-gather(bf16[1,32,128]{2,1,0:T(8,128)(2,1)S(1)} %get-tuple-element.151), channel_id=3, replica_groups=mesh['sp'=32,'tp'=4] {'sp'}, dimensions={1}, use_global_device_ids=true | all-gather | bytes 270336 | tf_op jit(solution)/shard_map/all_gather | solution.py:34
  68.6 2.3 collective-permute-start.3
  72.2 26.7 %all-gather.2 = bf16[1,128,1024]{1,2,0:T(8,128)(2,1)S(1)} all-gather(bf16[1,128,32]{1,2,0:T(8,128)(2,1)S(1)} %get-tuple-element.157), channel_id=4, replica_groups=mesh['sp'=32,'tp'=4] {'sp'}, dimensions={2}, use_global_device_ids=true | all-gather | bytes 270336 | tf_op jit(solution)/shard_map/all_gather | solution.py:60
  99.6 10.7 %psum.28 = f32[512]{0:T(512)S(1)} all-reduce(f32[512]{0:T(512)S(1)} %pad_maximum_fusion.4), channel_id=1, replica_groups=mesh['sp'=32,'tp'=4] {'tp'}, use_global_device_ids=true, to_apply=%region_3.4 | all-reduce | flops 512 | bytes 4096 | tf_op jit(solution)/shard_map/psum | solution.py:55
  111.7 18.6 %reduce-scatter.5.cloned.1.call-done = bf16[4,64,256]{2,1,0:T(8,128)(2,1)} async-done(((bf16[4,64,1024]{2,1,0:T(8,128)(2,1)}), bf16[4,64,256]{2,1,0:T(8,128)(2,1)}) %reduce-scatter.5.cloned.1.call-update) | async-done | bytes 131088 | tf_op jit(solution)/shard_map/reduce_scatter | solution.py:131
  131.3 3.2 collective-permute-start.7
  134.6 2.9 collective-permute-done.5
  137.5 25.6 %all-gather.3 = bf16[1,1024,128]{2,1,0:T(8,128)(2,1)S(1)} all-gather(bf16[1,32,128]{2,1,0:T(8,128)(2,1)S(1)} %get-tuple-element.154), channel_id=5, replica_groups=mesh['sp'=32,'tp'=4] {'sp'}, dimensions={1}, use_global_device_ids=true | all-gather | bytes 270336 | tf_op jit(solution)/shard_map/all_gather | solution.py:34
  163.1 24.2 %all-gather.4 = bf16[1,1024,128]{2,1,0:T(8,128)(2,1)S(1)} all-gather(bf16[1,32,128]{2,1,0:T(8,128)(2,1)S(1)} %get-tuple-element.150), channel_id=6, replica_groups=mesh['sp'=32,'tp'=4] {'sp'}, dimensions={1}, use_global_device_ids=true | all-gather | bytes 270336 | tf_op jit(solution)/shard_map/all_gather | solution.py:34
  190.0 2.3 collective-permute-start.8
  193.5 26.8 %all-gather.5 = bf16[1,128,1024]{1,2,0:T(8,128)(2,1)S(1)} all-gather(bf16[1,128,32]{1,2,0:T(8,128)(2,1)S(1)} %get-tuple-element.158), channel_id=7, replica_groups=mesh['sp'=32,'tp'=4] {'sp'}, dimensions={2}, use_global_device_ids=true | all-gather | bytes 270336 | tf_op jit(solution)/shard_map/all_gather | solution.py:60
  221.1 10.9 %psum.29 = f32[512]{0:T(512)S(1)} all-reduce(f32[512]{0:T(512)S(1)} %pad_maximum_fusion.5), channel_id=1, replica_groups=mesh['sp'=32,'tp'=4] {'tp'}, use_global_device_ids=true, to_apply=%region_8.9 | all-reduce | flops 512 | bytes 4096 | tf_op jit(solution)/shard_map/psum | solution.py:55
  233.4 18.5 %reduce-scatter.7.cloned.1.call-done = bf16[4,64,256]{2,1,0:T(8,128)(2,1)} async-done(((bf16[4,64,1024]{2,1,0:T(8,128)(2,1)}), bf16[4,64,256]{2,1,0:T(8,128)(2,1)}) %reduce-scatter.7.cloned.1.call-update) | async-done | bytes 131088 | tf_op jit(solution)/shard_map/reduce_scatter | solution.py:131
  253.0 3.3 collective-permute-start.12
  256.3 2.9 collective-permute-done.10
  259.2 25.1 %all-gather.6 = bf16[1,1024,128]{2,1,0:T(8,128)(2,1)S(1)} all-gather(bf16[1,32,128]{2,1,0:T(8,128)(2,1)S(1)} %get-tuple-element.156), channel_id=8, replica_groups=mesh['sp'=32,'tp'=4] {'sp'}, dimensions={1}, use_global_device_ids=true | all-gather | bytes 270336 | tf_op jit(solution)/shard_map/all_gather | solution.py:34
  284.3 24.4 %all-gather.7 = bf16[1,1024,128]{2,1,0:T(8,128)(2,1)S(1)} all-gather(bf16[1,32,128]{2,1,0:T(8,128)(2,1)S(1)} %get-tuple-element.152), channel_id=9, replica_groups=mesh['sp'=32,'tp'=4] {'sp'}, dimensions={1}, use_global_device_ids=true | all-gather | bytes 270336 | tf_op jit(solution)/shard_map/all_gather | solution.py:34
  311.3 2.3 collective-permute-start.13
  314.9 26.8 %all-gather.8 = bf16[1,128,1024]{1,2,0:T(8,128)(2,1)S(1)} all-gather(bf16[1,128,32]{1,2,0:T(8,128)(2,1)S(1)} %get-tuple-element.160), channel_id=10, replica_groups=mesh['sp'=32,'tp'=4] {'sp'}, dimensions={2}, use_global_device_ids=true | all-gather | bytes 270336 | tf_op jit(solution)/shard_map/all_gather | solution.py:60
  342.4 10.9 %psum.30 = f32[512]{0:T(512)S(1)} all-reduce(f32[512]{0:T(512)S(1)} %pad_maximum_fusion.6), channel_id=1, replica_groups=mesh['sp'=32,'tp'=4] {'tp'}, use_global_device_ids=true, to_apply=%region_13.14 | all-reduce | flops 512 | bytes 4096 | tf_op jit(solution)/shard_map/psum | solution.py:55
  354.8 18.5 %reduce-scatter.9.cloned.1.call-done = bf16[4,64,256]{2,1,0:T(8,128)(2,1)} async-done(((bf16[4,64,1024]{2,1,0:T(8,128)(2,1)}), bf16[4,64,256]{2,1,0:T(8,128)(2,1)}) %reduce-scatter.9.cloned.1.call-update) | async-done | bytes 131088 | tf_op jit(solution)/shard_map/reduce_scatter | solution.py:131
  374.3 3.2 collective-permute-start.17
  377.6 2.9 collective-permute-done.15
  380.5 25.1 %all-gather.9 = bf16[1,1024,128]{2,1,0:T(8,128)(2,1)S(1)} all-gather(bf16[1,32,128]{2,1,0:T(8,128)(2,1)S(1)} %get-tuple-element.155), channel_id=11, replica_groups=mesh['sp'=32,'tp'=4] {'sp'}, dimensions={1}, use_global_device_ids=true | all-gather | bytes 270336 | tf_op jit(solution)/shard_map/all_gather | solution.py:34
  405.6 24.4 %all-gather.10 = bf16[1,1024,128]{2,1,0:T(8,128)(2,1)S(1)} all-gather(bf16[1,32,128]{2,1,0:T(8,128)(2,1)S(1)} %get-tuple-element.149), channel_id=12, replica_groups=mesh['sp'=32,'tp'=4] {'sp'}, dimensions={1}, use_global_device_ids=true | all-gather | bytes 270336 | tf_op jit(solution)/shard_map/all_gather | solution.py:34
  432.7 2.3 collective-permute-start.18
  436.3 26.8 %all-gather.11 = bf16[1,128,1024]{1,2,0:T(8,128)(2,1)S(1)} all-gather(bf16[1,128,32]{1,2,0:T(8,128)(2,1)S(1)} %get-tuple-element.159), channel_id=13, replica_groups=mesh['sp'=32,'tp'=4] {'sp'}, dimensions={2}, use_global_device_ids=true | all-gather | bytes 270336 | tf_op jit(solution)/shard_map/all_gather | solution.py:60
  463.8 10.9 %psum.31 = f32[512]{0:T(512)S(1)} all-reduce(f32[512]{0:T(512)S(1)} %pad_maximum_fusion.7), channel_id=1, replica_groups=mesh['sp'=32,'tp'=4] {'tp'}, use_global_device_ids=true, to_apply=%region_18.19 | all-reduce | flops 512 | bytes 4096 | tf_op jit(solution)/shard_map/psum | solution.py:55
  476.1 18.6 %reduce-scatter.11.cloned.1.call-done = bf16[4,64,256]{2,1,0:T(8,128)(2,1)} async-done(((bf16[4,64,1024]{2,1,0:T(8,128)(2,1)}), bf16[4,64,256]{2,1,0:T(8,128)(2,1)}) %reduce-scatter.11.cloned.1.call-update) | async-done | bytes 131088 | tf_op jit(solution)/shard_map/reduce_scatter | solution.py:131
  (157 shorter events, 34.2 us)
Async XLA Ops:
  6.5 123.8 %reduce-scatter.5.cloned.1.call-start = ((), (), s32[]{:S(2)}) async-start(), calls=%async_computation.4 | async-start | bytes 655360 | tf_op jit(solution)/shard_map/reduce_scatter | solution.py:131
  6.5 34.6 %collective-permute-start = (bf16[4,64,256]{2,1,0:T(8,128)(2,1)}, bf16[4,64,256]{2,1,0:T(8,128)(2,1)S(1)}, u32[]{:S(2)}, u32[]{:S(2)}) collective-permute-start(bf16[4,64,256]{2,1,0:T(8,128)(2,1)} %param.9), channel_id=1, source_target_pairs={{0,1},{1,2},{2,3},{3,0},{4,5},{5,6},{6,7},{7,4},{8,9},{9,10},{10,1... | collective-permute-start | bytes 393224 | tf_op jit(solution)/shard_map/ppermute | solution.py:24
  8.1 57.7 %collective-permute-start.2 = (bf16[4,64,256]{2,1,0:T(8,128)(2,1)}, bf16[4,64,256]{2,1,0:T(8,128)(2,1)S(1)}, u32[]{:S(2)}, u32[]{:S(2)}) collective-permute-start(bf16[4,64,256]{2,1,0:T(8,128)(2,1)} %param.9), channel_id=1, source_target_pairs={{1,0},{2,1},{3,2},{0,3},{5,4},{6,5},{7,6},{4,7},{9,8},{10,9},{11,1... | collective-permute-start | bytes 393224 | tf_op jit(solution)/shard_map/ppermute | solution.py:26
  9.8 2.6 copy-start.5
  10.6 1.7 copy-start.2
  12.4 0.8 copy-start.3
  13.2 0.7 copy-start.6
  13.2 0.8 copy-start.4
  13.9 0.7 copy-start.8
  41.1 24.8 %collective-permute-start.1 = (bf16[4,64,256]{2,1,0:T(8,128)(2,1)S(1)}, bf16[4,64,256]{2,1,0:T(8,128)(2,1)S(1)}, u32[]{:S(2)}, u32[]{:S(2)}) collective-permute-start(bf16[4,64,256]{2,1,0:T(8,128)(2,1)S(1)} %collective-permute-done), channel_id=1, source_target_pairs={{0,1},{1,2},{2,3},{3,0},{4,5},{5,6},{6,7},{7,4},{8,9},{9,10},{10,1... | collective-permute-start | bytes 393224 | tf_op jit(solution)/shard_map/ppermute | solution.py:24
  41.5 24.4 %copy-start = (bf16[4,64,256]{2,1,0:T(8,128)(2,1)S(1)}, bf16[4,64,256]{2,1,0:T(8,128)(2,1)}, u32[]{:S(2)}) copy-start(bf16[4,64,256]{2,1,0:T(8,128)(2,1)} %param.9) | copy-start | bytes 393220
  68.6 30.3 %collective-permute-start.3 = (bf16[4,15,128]{2,1,0:T(8,128)(2,1)S(1)}, bf16[4,15,128]{2,1,0:T(8,128)(2,1)S(1)}, u32[]{:S(2)}, u32[]{:S(2)}) collective-permute-start(bf16[4,15,128]{2,1,0:T(8,128)(2,1)S(1)} %get-tuple-element.23), channel_id=1, source_target_pairs={{0,4},{4,8},{8,12},{12,16},{16,20},{20,24},{24,28},{28,32},{32,36}... | collective-permute-start | bytes 46088 | tf_op jit(solution)/shard_map/ppermute | solution.py:45
  70.9 28.0 %collective-permute-start.4 = (bf16[4,15,128]{2,1,0:T(8,128)(2,1)S(1)}, bf16[4,15,128]{2,1,0:T(8,128)(2,1)S(1)}, u32[]{:S(2)}, u32[]{:S(2)}) collective-permute-start(bf16[4,15,128]{2,1,0:T(8,128)(2,1)S(1)} %get-tuple-element.24), channel_id=1, source_target_pairs={{4,0},{8,4},{12,8},{16,12},{20,16},{24,20},{28,24},{32,28},{36,32}... | collective-permute-start | bytes 46088 | tf_op jit(solution)/shard_map/ppermute | solution.py:46
  111.7 25.8 %copy-start.1 = (f32[4,31,128]{2,0,1:T(4,128)S(1)}, f32[4,31,128]{2,0,1:T(4,128)}, u32[]{:S(2)}) copy-start(f32[4,31,128]{2,0,1:T(4,128)} %param.13) | copy-start | bytes 190468
  111.7 140.3 %reduce-scatter.7.cloned.1.call-start = ((), (), s32[]{:S(2)}) async-start(), calls=%async_computation.5 | async-start | bytes 655360 | tf_op jit(solution)/shard_map/reduce_scatter | solution.py:131
  131.2 6.2 %collective-permute-start.5 = (bf16[4,64,256]{2,1,0:T(8,128)(2,1)S(1)}, bf16[4,64,256]{2,1,0:T(8,128)(2,1)S(1)}, u32[]{:S(2)}, u32[]{:S(2)}) collective-permute-start(bf16[4,64,256]{2,1,0:T(8,128)(2,1)S(1)} %add_convert_fusion.3), channel_id=1, source_target_pairs={{0,1},{1,2},{2,3},{3,0},{4,5},{5,6},{6,7},{7,4},{8,9},{9,10},{10,1... | collective-permute-start | bytes 393224 | tf_op jit(solution)/shard_map/ppermute | solution.py:24
  131.3 56.0 %collective-permute-start.7 = (bf16[4,64,256]{2,1,0:T(8,128)(2,1)S(1)}, bf16[4,64,256]{2,1,0:T(8,128)(2,1)S(1)}, u32[]{:S(2)}, u32[]{:S(2)}) collective-permute-start(bf16[4,64,256]{2,1,0:T(8,128)(2,1)S(1)} %add_convert_fusion.3), channel_id=1, source_target_pairs={{1,0},{2,1},{3,2},{0,3},{5,4},{6,5},{7,6},{4,7},{9,8},{10,9},{11,1... | collective-permute-start | bytes 393224 | tf_op jit(solution)/shard_map/ppermute | solution.py:26
  137.5 49.8 %collective-permute-start.6 = (bf16[4,64,256]{2,1,0:T(8,128)(2,1)S(1)}, bf16[4,64,256]{2,1,0:T(8,128)(2,1)S(1)}, u32[]{:S(2)}, u32[]{:S(2)}) collective-permute-start(bf16[4,64,256]{2,1,0:T(8,128)(2,1)S(1)} %collective-permute-done.5), channel_id=1, source_target_pairs={{0,1},{1,2},{2,3},{3,0},{4,5},{5,6},{6,7},{7,4},{8,9},{9,10},{10,1... | collective-permute-start | bytes 393224 | tf_op jit(solution)/shard_map/ppermute | solution.py:24
  190.0 30.3 %collective-permute-start.8 = (bf16[4,15,128]{2,1,0:T(8,128)(2,1)S(1)}, bf16[4,15,128]{2,1,0:T(8,128)(2,1)S(1)}, u32[]{:S(2)}, u32[]{:S(2)}) collective-permute-start(bf16[4,15,128]{2,1,0:T(8,128)(2,1)S(1)} %get-tuple-element.21), channel_id=1, source_target_pairs={{0,4},{4,8},{8,12},{12,16},{16,20},{20,24},{24,28},{28,32},{32,36}... | collective-permute-start | bytes 46088 | tf_op jit(solution)/shard_map/ppermute | solution.py:45
  192.2 28.1 %collective-permute-start.9 = (bf16[4,15,128]{2,1,0:T(8,128)(2,1)S(1)}, bf16[4,15,128]{2,1,0:T(8,128)(2,1)S(1)}, u32[]{:S(2)}, u32[]{:S(2)}) collective-permute-start(bf16[4,15,128]{2,1,0:T(8,128)(2,1)S(1)} %get-tuple-element.22), channel_id=1, source_target_pairs={{4,0},{8,4},{12,8},{16,12},{20,16},{24,20},{28,24},{32,28},{36,32}... | collective-permute-start | bytes 46088 | tf_op jit(solution)/shard_map/ppermute | solution.py:46
  233.4 139.9 %reduce-scatter.9.cloned.1.call-start = ((), (), s32[]{:S(2)}) async-start(), calls=%async_computation.6 | async-start | bytes 655360 | tf_op jit(solution)/shard_map/reduce_scatter | solution.py:131
  252.9 6.2 %collective-permute-start.10 = (bf16[4,64,256]{2,1,0:T(8,128)(2,1)S(1)}, bf16[4,64,256]{2,1,0:T(8,128)(2,1)S(1)}, u32[]{:S(2)}, u32[]{:S(2)}) collective-permute-start(bf16[4,64,256]{2,1,0:T(8,128)(2,1)S(1)} %add_convert_fusion.2), channel_id=1, source_target_pairs={{0,1},{1,2},{2,3},{3,0},{4,5},{5,6},{6,7},{7,4},{8,9},{9,10},{10,1... | collective-permute-start | bytes 393224 | tf_op jit(solution)/shard_map/ppermute | solution.py:24
  253.0 55.6 %collective-permute-start.12 = (bf16[4,64,256]{2,1,0:T(8,128)(2,1)S(1)}, bf16[4,64,256]{2,1,0:T(8,128)(2,1)S(1)}, u32[]{:S(2)}, u32[]{:S(2)}) collective-permute-start(bf16[4,64,256]{2,1,0:T(8,128)(2,1)S(1)} %add_convert_fusion.2), channel_id=1, source_target_pairs={{1,0},{2,1},{3,2},{0,3},{5,4},{6,5},{7,6},{4,7},{9,8},{10,9},{11,1... | collective-permute-start | bytes 393224 | tf_op jit(solution)/shard_map/ppermute | solution.py:26
  259.1 49.5 %collective-permute-start.11 = (bf16[4,64,256]{2,1,0:T(8,128)(2,1)S(1)}, bf16[4,64,256]{2,1,0:T(8,128)(2,1)S(1)}, u32[]{:S(2)}, u32[]{:S(2)}) collective-permute-start(bf16[4,64,256]{2,1,0:T(8,128)(2,1)S(1)} %collective-permute-done.10), channel_id=1, source_target_pairs={{0,1},{1,2},{2,3},{3,0},{4,5},{5,6},{6,7},{7,4},{8,9},{9,10},{10,1... | collective-permute-start | bytes 393224 | tf_op jit(solution)/shard_map/ppermute | solution.py:24
  311.3 30.3 %collective-permute-start.13 = (bf16[4,15,128]{2,1,0:T(8,128)(2,1)S(1)}, bf16[4,15,128]{2,1,0:T(8,128)(2,1)S(1)}, u32[]{:S(2)}, u32[]{:S(2)}) collective-permute-start(bf16[4,15,128]{2,1,0:T(8,128)(2,1)S(1)} %get-tuple-element.19), channel_id=1, source_target_pairs={{0,4},{4,8},{8,12},{12,16},{16,20},{20,24},{24,28},{28,32},{32,36}... | collective-permute-start | bytes 46088 | tf_op jit(solution)/shard_map/ppermute | solution.py:45
  313.6 28.1 %collective-permute-start.14 = (bf16[4,15,128]{2,1,0:T(8,128)(2,1)S(1)}, bf16[4,15,128]{2,1,0:T(8,128)(2,1)S(1)}, u32[]{:S(2)}, u32[]{:S(2)}) collective-permute-start(bf16[4,15,128]{2,1,0:T(8,128)(2,1)S(1)} %get-tuple-element.20), channel_id=1, source_target_pairs={{4,0},{8,4},{12,8},{16,12},{20,16},{24,20},{28,24},{32,28},{36,32}... | collective-permute-start | bytes 46088 | tf_op jit(solution)/shard_map/ppermute | solution.py:46
  354.8 140.0 %reduce-scatter.11.cloned.1.call-start = ((), (), s32[]{:S(2)}) async-start(), calls=%async_computation.7 | async-start | bytes 655360 | tf_op jit(solution)/shard_map/reduce_scatter | solution.py:131
  374.3 6.2 %collective-permute-start.15 = (bf16[4,64,256]{2,1,0:T(8,128)(2,1)S(1)}, bf16[4,64,256]{2,1,0:T(8,128)(2,1)S(1)}, u32[]{:S(2)}, u32[]{:S(2)}) collective-permute-start(bf16[4,64,256]{2,1,0:T(8,128)(2,1)S(1)} %add_convert_fusion.1), channel_id=1, source_target_pairs={{0,1},{1,2},{2,3},{3,0},{4,5},{5,6},{6,7},{7,4},{8,9},{9,10},{10,1... | collective-permute-start | bytes 393224 | tf_op jit(solution)/shard_map/ppermute | solution.py:24
  374.3 55.7 %collective-permute-start.17 = (bf16[4,64,256]{2,1,0:T(8,128)(2,1)S(1)}, bf16[4,64,256]{2,1,0:T(8,128)(2,1)S(1)}, u32[]{:S(2)}, u32[]{:S(2)}) collective-permute-start(bf16[4,64,256]{2,1,0:T(8,128)(2,1)S(1)} %add_convert_fusion.1), channel_id=1, source_target_pairs={{1,0},{2,1},{3,2},{0,3},{5,4},{6,5},{7,6},{4,7},{9,8},{10,9},{11,1... | collective-permute-start | bytes 393224 | tf_op jit(solution)/shard_map/ppermute | solution.py:26
  380.5 49.5 %collective-permute-start.16 = (bf16[4,64,256]{2,1,0:T(8,128)(2,1)S(1)}, bf16[4,64,256]{2,1,0:T(8,128)(2,1)S(1)}, u32[]{:S(2)}, u32[]{:S(2)}) collective-permute-start(bf16[4,64,256]{2,1,0:T(8,128)(2,1)S(1)} %collective-permute-done.15), channel_id=1, source_target_pairs={{0,1},{1,2},{2,3},{3,0},{4,5},{5,6},{6,7},{7,4},{8,9},{9,10},{10,1... | collective-permute-start | bytes 393224 | tf_op jit(solution)/shard_map/ppermute | solution.py:24
  432.7 30.3 %collective-permute-start.18 = (bf16[4,15,128]{2,1,0:T(8,128)(2,1)S(1)}, bf16[4,15,128]{2,1,0:T(8,128)(2,1)S(1)}, u32[]{:S(2)}, u32[]{:S(2)}) collective-permute-start(bf16[4,15,128]{2,1,0:T(8,128)(2,1)S(1)} %get-tuple-element.17), channel_id=1, source_target_pairs={{0,4},{4,8},{8,12},{12,16},{16,20},{20,24},{24,28},{28,32},{32,36}... | collective-permute-start | bytes 46088 | tf_op jit(solution)/shard_map/ppermute | solution.py:45
  435.0 28.1 %collective-permute-start.19 = (bf16[4,15,128]{2,1,0:T(8,128)(2,1)S(1)}, bf16[4,15,128]{2,1,0:T(8,128)(2,1)S(1)}, u32[]{:S(2)}, u32[]{:S(2)}) collective-permute-start(bf16[4,15,128]{2,1,0:T(8,128)(2,1)S(1)} %get-tuple-element.18), channel_id=1, source_target_pairs={{4,0},{8,4},{12,8},{16,12},{20,16},{24,20},{28,24},{32,28},{36,32}... | collective-permute-start | bytes 46088 | tf_op jit(solution)/shard_map/ppermute | solution.py:46
  (1 other events, 0.7 us)
Sparse Core Ops, SparseCore 0:
  111.8 18.4 reduce-scatter.4
  233.5 18.3 reduce-scatter.6
  354.9 18.3 reduce-scatter.8
  476.3 18.3 reduce-scatter.10
